TPU v7x, 32 devices: a whole 2x2x4 slice. The times are simulated.
32 devices in a mesh: ep: 8 (over z, core), tp: 4 (over y, x).
Axes of the slice: x: 2, y: 2, z: 4, core: 2. Of those that a mesh axis runs over, the one named last changes fastest.
Arguments:
- tokens: bfloat16 [256, 4096], P('ep'), may hold values from -6 to 6
- recur_state: float32 [256, 4096], P('ep', 'tp'), may hold values from -6 to 6
- conv_state: bfloat16 [256, 3, 4096], P('ep', None, 'tp'), may hold values from -6 to 6
- mix_gain: float32 [4096], replicated, may hold values from 0.1 to 1.9
- in_weight: bfloat16 [4096, 4096], P('ep', 'tp'), may hold values from -0.09375 to 0.09375
- gate_weight: bfloat16 [4096, 4096], P('ep', 'tp'), may hold values from -0.09375 to 0.09375
- conv_taps: float32 [4, 4096], P(None, 'tp'), may hold values from -3 to 3
- recur_gate_blocks: bfloat16 [64, 64, 64], P('tp'), may hold values from -0.75 to 0.75
- input_gate_blocks: bfloat16 [64, 64, 64], P('tp'), may hold values from -0.75 to 0.75
- decay_rate: float32 [4096], P('tp'), may hold values from 0.01 to 0.4
- out_weight: bfloat16 [4096, 4096], P('tp', 'ep'), may hold values from -0.09375 to 0.09375
- ffn_gain: float32 [4096], replicated, may hold values from 0.1 to 1.9
- router_weight: bfloat16 [4096, 8], replicated, may hold values from -0.09375 to 0.09375
- routes: int32 [256, 2], P('ep'), may hold values from 0 to 7, as said below
- expert_gate: bfloat16 [8, 4096, 2048], P('ep', None, 'tp'), may hold values from -0.09375 to 0.09375
- expert_up: bfloat16 [8, 4096, 2048], P('ep', None, 'tp'), may hold values from -0.09375 to 0.09375
- expert_down: bfloat16 [8, 2048, 4096], P('ep', 'tp'), may hold values from -0.125 to 0.125
- dense_gate: bfloat16 [4096, 2048], P('ep', 'tp'), may hold values from -0.09375 to 0.09375
- dense_up: bfloat16 [4096, 2048], P('ep', 'tp'), may hold values from -0.09375 to 0.09375
- dense_down: bfloat16 [2048, 4096], P('tp', 'ep'), may hold values from -0.125 to 0.125
- branch_gate: bfloat16 [4096], replicated, may hold values from -0.09375 to 0.09375
Outputs:
- layer_out: bfloat16 [256, 4096], P('ep')
- new_state: float32 [256, 4096], P('ep', 'tp')
- new_conv_state: bfloat16 [256, 3, 4096], P('ep', None, 'tp')
Inputs may be any that keep to these rules, and one draw needn't show every extreme that they name: `routes`: A row names two different experts of one group: both have the same e // 4. In the rows of one index of ep no expert is named more than 16 times, and in every draw some expert is named exactly 16 times by the rows of every index of ep.
All inputs are finite; a program needn't handle non-finite values.
Results may differ from a plain program's by a relative error of at most 0.023.
Values may be sent and summed in bfloat16 or wider, within the bound.
A program may use at most 64 MiB of HBM per device.

v0:
```python
import jax
import jax.numpy as jnp
from jax import lax
from jax.sharding import PartitionSpec as P

TOP_K = 2
epsilon = 1e-06
decay_scale = 8.0


def rms_scale(rows, gain):
    values = rows.astype(jnp.float32)
    inverse = lax.rsqrt(jnp.mean(values * values, axis=-1, keepdims=True) + epsilon)
    return (values * inverse * gain).astype(jnp.bfloat16)


def on_device(
    tokens,
    recur_state,
    conv_state,
    mix_gain,
    in_weight,
    gate_weight,
    conv_taps,
    recur_gate_blocks,
    input_gate_blocks,
    decay_rate,
    out_weight,
    ffn_gain,
    router_weight,
    routes,
    expert_gate,
    expert_up,
    expert_down,
    dense_gate,
    dense_up,
    dense_down,
    branch_gate,
):
    batch_rows, width = tokens.shape
    channels = in_weight.shape[1]
    normed = rms_scale(tokens, mix_gain)
    arrived = lax.all_to_all(normed, "ep", split_axis=1, concat_axis=0, tiled=True)
    joined = jnp.concatenate([in_weight, gate_weight], axis=1)
    summed = lax.psum_scatter(
        jnp.dot(arrived, joined, preferred_element_type=jnp.float32).astype(jnp.bfloat16),
        "ep",
        scatter_dimension=0,
        tiled=True,
    ).astype(jnp.float32)
    x_sum, gate_sum = (summed[:, :channels], summed[:, channels:])
    x_branch = x_sum.astype(jnp.bfloat16)
    gate_branch = gate_sum.astype(jnp.bfloat16)
    window = jnp.concatenate([conv_state, x_branch[:, None, :]], axis=1)
    conv_out = jnp.sum(window.astype(jnp.float32) * conv_taps[None], axis=1).astype(jnp.bfloat16)
    new_conv_state = window[:, 1:, :]
    blocks = conv_out.reshape(batch_rows, recur_gate_blocks.shape[0], recur_gate_blocks.shape[1])
    recur_gate = jax.nn.sigmoid(
        jnp.einsum(
            "bhi,hij->bhj", blocks, recur_gate_blocks, preferred_element_type=jnp.float32
        ).reshape(batch_rows, channels)
    )
    input_gate = jax.nn.sigmoid(
        jnp.einsum(
            "bhi,hij->bhj", blocks, input_gate_blocks, preferred_element_type=jnp.float32
        ).reshape(batch_rows, channels)
    )
    log_decay = -decay_scale * recur_gate * decay_rate
    new_state = jnp.exp(log_decay) * recur_state + jnp.sqrt(
        -jnp.expm1(2.0 * log_decay)
    ) * input_gate * conv_out.astype(jnp.float32)
    mixer_rows = (new_state * jax.nn.gelu(gate_branch.astype(jnp.float32))).astype(jnp.bfloat16)
    mixer_part = jnp.dot(
        mixer_rows,
        lax.all_gather(out_weight, "ep", axis=1, tiled=True),
        preferred_element_type=jnp.float32,
    )
    resid = (
        tokens.astype(jnp.float32)
        + lax.psum(mixer_part.astype(jnp.bfloat16), "tp").astype(jnp.float32)
    ).astype(jnp.bfloat16)
    normed_ffn = rms_scale(resid, ffn_gain)
    router_logits = jnp.dot(normed_ffn, router_weight, preferred_element_type=jnp.float32)
    experts = router_logits.shape[1]
    expert_ids = lax.broadcasted_iota(jnp.int32, (batch_rows, TOP_K, experts), 2)
    picked = jnp.sum(
        jnp.where(routes[:, :, None] == expert_ids, router_logits[:, None, :], 0.0), axis=2
    )
    route_weight = jax.nn.sigmoid(picked - picked[:, ::-1]).astype(jnp.bfloat16)
    capacity = 2 * batch_rows * TOP_K // experts
    flat_ids = routes.reshape(batch_rows * TOP_K)
    onehot = (
        flat_ids[:, None] == lax.broadcasted_iota(jnp.int32, (batch_rows * TOP_K, experts), 1)
    ).astype(jnp.int32)
    rank = jnp.sum((jnp.cumsum(onehot, axis=0) - onehot) * onehot, axis=1)
    slot_of = (flat_ids * capacity + rank).reshape(batch_rows, TOP_K)
    slot_rows = lax.broadcasted_iota(jnp.int32, (experts * capacity, batch_rows), 0)
    slot_cols = lax.broadcasted_iota(jnp.int32, (batch_rows, experts * capacity), 1)
    dispatch = jnp.zeros((experts * capacity, batch_rows), jnp.bfloat16)
    combine = jnp.zeros((batch_rows, experts * capacity), jnp.bfloat16)
    for pick in range(TOP_K):
        dispatch = dispatch + (slot_rows == slot_of[None, :, pick]).astype(jnp.bfloat16)
        combine = combine + jnp.where(
            slot_cols == slot_of[:, pick : pick + 1],
            route_weight[:, pick : pick + 1],
            jnp.zeros((), jnp.bfloat16),
        )
    outgoing = (
        jnp.dot(dispatch, normed_ffn, preferred_element_type=jnp.float32)
        .astype(jnp.bfloat16)
        .reshape(experts, capacity, width)
    )
    gate_local = expert_gate[0]
    up_local = expert_up[0]
    down_local = expert_down[0]
    arrived_rows = lax.all_to_all(outgoing, "ep", split_axis=0, concat_axis=0, tiled=True)
    sources, items, features = arrived_rows.shape
    rows = arrived_rows.reshape(sources * items, features)
    first = jnp.dot(rows, gate_local, preferred_element_type=jnp.float32)
    second = jnp.dot(rows, up_local, preferred_element_type=jnp.float32)
    act = (jax.nn.silu(first) * second).astype(jnp.bfloat16)
    partial_value = jnp.dot(act, down_local, preferred_element_type=jnp.float32)
    total = lax.psum(partial_value.astype(jnp.bfloat16), "tp")
    returned = lax.all_to_all(
        total.reshape(sources, items, total.shape[1]), "ep", split_axis=0, concat_axis=0, tiled=True
    )
    moe = jnp.dot(
        combine,
        returned.reshape(experts * capacity, returned.shape[2]),
        preferred_element_type=jnp.float32,
    )
    dense_arrived = lax.all_to_all(normed_ffn, "ep", split_axis=1, concat_axis=0, tiled=True)
    dense_joined = jnp.concatenate([dense_gate, dense_up], axis=1)
    dense_summed = lax.psum_scatter(
        jnp.dot(dense_arrived, dense_joined, preferred_element_type=jnp.float32).astype(
            jnp.bfloat16
        ),
        "ep",
        scatter_dimension=0,
        tiled=True,
    ).astype(jnp.float32)
    dense_first = dense_summed[:, : dense_gate.shape[1]]
    dense_second = dense_summed[:, dense_gate.shape[1] :]
    dense_act = (jax.nn.silu(dense_first) * dense_second).astype(jnp.bfloat16)
    dense_part = jnp.dot(
        dense_act,
        lax.all_gather(dense_down, "ep", axis=1, tiled=True),
        preferred_element_type=jnp.float32,
    )
    branch_weight = jax.nn.sigmoid(
        jnp.dot(normed_ffn, branch_gate, preferred_element_type=jnp.float32)
    )
    dense_sum = lax.psum(dense_part.astype(jnp.bfloat16), "tp").astype(jnp.float32)
    layer_out = (resid.astype(jnp.float32) + moe + branch_weight[:, None] * dense_sum).astype(
        jnp.bfloat16
    )
    return (layer_out, new_state, new_conv_state)


def solution(mesh):
    in_specs = (
        P("ep", None),
        P("ep", "tp"),
        P("ep", None, "tp"),
        P(),
        P("ep", "tp"),
        P("ep", "tp"),
        P(None, "tp"),
        P("tp", None, None),
        P("tp", None, None),
        P("tp"),
        P("tp", "ep"),
        P(),
        P(),
        P("ep", None),
        P("ep", None, "tp"),
        P("ep", None, "tp"),
        P("ep", "tp", None),
        P("ep", "tp"),
        P("ep", "tp"),
        P("tp", "ep"),
        P(),
    )
    out_specs = (P("ep", None), P("ep", "tp"), P("ep", None, "tp"))
    return jax.shard_map(
        on_device, mesh=mesh, in_specs=in_specs, out_specs=out_specs, check_vma=False
    )
```

profile of v0, /device:TPU:0, one launch (start us, length us, event | category | flops | bytes accessed | tf_op | source)
XLA Modules:
  0.0 396.9 jit_solution(11186199223250125864)
XLA Ops:
  7.2 1.1 fusion.33
  8.4 1.1 fusion.35
  9.5 16.0 %all_to_all.48 = bf16[32,8,512]{2,0,1:T(8,128)(2,1)S(1)} all-to-all(bf16[32,8,512]{2,0,1:T(8,128)(2,1)S(1)} %bitcast.77), channel_id=1, replica_groups=mesh['ep'=8,'tp'=4] {'ep'}, dimensions={1} | all-to-all | bytes 524288 | tf_op jit(solution)/shard_map/all_to_all | solution.py:43
  25.5 3.4 convolution_convert_fusion.4
  29.0 0.7 all-gather.3.cloned.1.call-update
  29.8 30.9 %reduce-scatter.3.cloned.1.call-done = bf16[32,2048]{1,0:T(8,128)(2,1)} async-done(((bf16[256,2048]{1,0:T(8,128)(2,1)}), bf16[32,2048]{1,0:T(8,128)(2,1)}) %reduce-scatter.3.cloned.1.call-update) | async-done | bytes 131088 | tf_op jit(solution)/shard_map/reduce_scatter | solution.py:45
  60.7 0.9 slice_bitcast_fusion
  61.9 0.2 fusion.17
  62.4 0.2 fusion.13
  63.1 79.5 %all-gather.3.cloned.1.call-done = bf16[1024,4096]{1,0:T(8,128)(2,1)} async-done(((bf16[1024,512]{1,0:T(8,128)(2,1)}), bf16[1024,4096]{1,0:T(8,128)(2,1)}) %all-gather.3.cloned.1.call-update) | async-done | bytes 8388624 | tf_op jit(solution)/shard_map/all_gather | solution.py:75
  142.5 5.6 %convolution_convert_fusion.3 = bf16[32,4096]{1,0:T(8,128)(2,1)} fusion(bf16[1024,4096]{1,0:T(8,128)(2,1)} %all-gather.3.cloned.1.call-done, f32[32,1024]{1,0:T(8,128)S(1)} %multiply_add_fusion, bf16[32,2048]{1,0:T(8,128)(2,1)S(1)} %copy-done.5), kind=kOutput, calls=%fused_computation.6 | convolution fusion | flops 268926976 | bytes 8847360 | tf_op jit(solution)/shard_map/dot_general | solution.py:73
  148.2 41.6 %all-reduce.4.cloned.1.call-done = bf16[32,4096]{1,0:T(8,128)(2,1)} async-done(((bf16[32,4096]{1,0:T(8,128)(2,1)}), bf16[32,4096]{1,0:T(8,128)(2,1)}) %all-reduce.4.cloned.1.call-update) | async-done | bytes 262160 | tf_op jit(solution)/shard_map/psum | solution.py:80
  189.9 1.1 fusion.37
  191.0 1.1 fusion.39
  192.1 14.1 %all_to_all.49 = bf16[32,8,512]{2,0,1:T(8,128)(2,1)S(1)} all-to-all(bf16[32,8,512]{2,0,1:T(8,128)(2,1)S(1)} %bitcast.78), channel_id=1, replica_groups=mesh['ep'=8,'tp'=4] {'ep'}, dimensions={1} | all-to-all | bytes 524288 | tf_op jit(solution)/shard_map/all_to_all | solution.py:132
  206.2 1.3 convolution_convert_fusion.5
  207.6 0.5 all-gather.5.cloned.1.call-update
  208.5 0.2 select_reduce_fusion
  208.9 1.4 convolution_convert_fusion.1
  210.3 3.6 all-to-all-start.1
  213.9 24.5 %reduce-scatter.5.cloned.1.call-done = bf16[32,1024]{1,0:T(8,128)(2,1)} async-done(((bf16[256,1024]{1,0:T(8,128)(2,1)}), bf16[32,1024]{1,0:T(8,128)(2,1)}) %reduce-scatter.5.cloned.1.call-update) | async-done | bytes 65552 | tf_op jit(solution)/shard_map/reduce_scatter | solution.py:134
  238.4 0.8 convert_element_type.109
  239.2 49.8 %all-gather.5.cloned.1.call-done = bf16[512,4096]{1,0:T(8,128)(2,1)} async-done(((bf16[512,512]{1,0:T(8,128)(2,1)}), bf16[512,4096]{1,0:T(8,128)(2,1)}) %all-gather.5.cloned.1.call-update) | async-done | bytes 4194320 | tf_op jit(solution)/shard_map/all_gather | solution.py:147
  289.0 3.7 convolution_convert_fusion.2
  292.7 2.9 fusion.5
  295.7 5.9 %convolution_convert_fusion = bf16[128,4096]{1,0:T(8,128)(2,1)} fusion(bf16[1,512,4096]{2,1,0:T(8,128)(2,1)} %param.37, bf16[128,4096]{1,0:T(8,128)(2,1)S(1)} %bitcast.72, bf16[1,4096,512]{2,1,0:T(8,128)(2,1)} %param.36, f32[128,512]{1,0:T(8,128)S(1)} %fusion.5), kind=kOutput, calls=%fused_computation | convolution fusion | flops 1074659328 | bytes 10747904 | tf_op jit(solution)/shard_map/dot_general | solution.py:122
  301.6 55.4 %all-reduce.6.cloned.1.call-done = (bf16[8,16,4096]{2,1,0:T(8,128)(2,1)}, bf16[32,4096]{1,0:T(8,128)(2,1)}) async-done(((bf16[8,16,4096]{2,1,0:T(8,128)(2,1)}, bf16[32,4096]{1,0:T(8,128)(2,1)}), (bf16[8,16,4096]{2,1,0:T(8,128)(2,1)}, bf16[32,4096]{1,0:T(8,128)(2,1)})) %all-reduce.6.cloned.1.call-update) | async-done | bytes 1310736 | tf_op jit(solution)/shard_map/psum | solution.py:123
  356.9 4.6 %all-to-all-start.2 = ((bf16[8,16,4096]{2,1,0:T(8,128)(2,1)}), bf16[8,16,4096]{2,1,0:T(8,128)(2,1)S(1)}, u32[]{:S(2)}, u32[]{:S(2)}) async-start(bf16[8,16,4096]{2,1,0:T(8,128)(2,1)} %get-tuple-element.3), calls=%async_computation.3 | async-start | bytes 2097152 | tf_op jit(solution)/shard_map/all_to_all | solution.py:124
  361.5 0.7 fusion.45
  362.5 0.2 fusion.27
  362.7 25.4 %all-to-all-done.2 = bf16[8,16,4096]{2,1,0:T(8,128)(2,1)S(1)} async-done(((bf16[8,16,4096]{2,1,0:T(8,128)(2,1)}), bf16[8,16,4096]{2,1,0:T(8,128)(2,1)S(1)}, u32[]{:S(2)}, u32[]{:S(2)}) %all-to-all-start.2) | async-done | bytes 1048608 | tf_op jit(solution)/shard_map/all_to_all | solution.py:124
  388.1 2.0 fusion.1
  (69 shorter events, 2.2 us)
Async XLA Ops:
  7.2 54.7 %copy-start = (bf16[16,64,64]{2,1,0:T(8,128)(2,1)S(1)}, bf16[16,64,64]{2,1,0:T(8,128)(2,1)}, u32[]{:S(2)}) copy-start(bf16[16,64,64]{2,1,0:T(8,128)(2,1)} %param.28) | copy-start | bytes 393220
  7.2 53.5 %reduce-scatter.3.cloned.1.call-start = ((), (), s32[]{:S(2)}) async-start(), calls=%async_computation.6 | async-start | bytes 1179648 | tf_op jit(solution)/shard_map/reduce_scatter | solution.py:45
  8.4 21.4 %copy-start.12 = (f32[1024]{0:T(1024)S(1)}, f32[1024]{0:T(1024)}, u32[]{:S(2)}) copy-start(f32[1024]{0:T(1024)} %param.30) | copy-start | bytes 12292
  9.5 52.1 %copy-start.4 = (bf16[32,3,1024]{2,0,1:T(8,128)(2,1)S(1)}, bf16[32,3,1024]{2,0,1:T(8,128)(2,1)}, u32[]{:S(2)}) copy-start(bf16[32,3,1024]{2,0,1:T(8,128)(2,1)} %param.23) | copy-start | bytes 589828
  9.5 52.1 %copy-start.9 = (f32[4,1024]{1,0:T(4,128)S(1)}, f32[4,1024]{1,0:T(4,128)}, u32[]{:S(2)}) copy-start(f32[4,1024]{1,0:T(4,128)} %param.27) | copy-start | bytes 49156
  25.5 36.8 %copy-start.15 = (bf16[16,64,64]{2,1,0:T(8,128)(2,1)S(1)}, bf16[16,64,64]{2,1,0:T(8,128)(2,1)}, u32[]{:S(2)}) copy-start(bf16[16,64,64]{2,1,0:T(8,128)(2,1)} %param.29) | copy-start | bytes 393220
  28.9 34.0 %copy-start.6 = (f32[32,1024]{1,0:T(8,128)S(1)}, f32[32,1024]{1,0:T(8,128)}, u32[]{:S(2)}) copy-start(f32[32,1024]{1,0:T(8,128)} %param.22) | copy-start | bytes 393220
  28.9 113.6 %all-gather.3.cloned.1.call-start = ((), (), s32[]{:S(2)}) async-start(), calls=%async_computation.7 | async-start | bytes 9437184 | tf_op jit(solution)/shard_map/all_gather | solution.py:75
  29.7 160.2 %all-reduce.4.cloned.1.call-start = ((), (), s32[]{:S(2)}) async-start(), calls=%async_computation.8 | async-start | bytes 524288 | tf_op jit(solution)/shard_map/psum | solution.py:80
  60.7 81.8 %copy-start.5 = (bf16[32,2048]{1,0:T(8,128)(2,1)S(1)}, bf16[32,2048]{1,0:T(8,128)(2,1)}, u32[]{:S(2)}) copy-start(bf16[32,2048]{1,0:T(8,128)(2,1)} %reduce-scatter.3.cloned.1.call-done) | copy-start | bytes 393220
  63.0 85.1 %copy-start.3 = (f32[32,1024]{1,0:T(8,128)}, f32[32,1024]{1,0:T(8,128)S(1)}, u32[]{:S(2)}) copy-start(f32[32,1024]{1,0:T(8,128)S(1)} %multiply_add_fusion) | copy-start | bytes 393220
  63.0 126.8 %copy-start.1 = (bf16[32,4096]{1,0:T(8,128)(2,1)S(1)}, bf16[32,4096]{1,0:T(8,128)(2,1)}, u32[]{:S(2)}) copy-start(bf16[32,4096]{1,0:T(8,128)(2,1)} %param.21) | copy-start | bytes 786436
  63.0 128.0 %copy-start.8 = (f32[4096]{0:T(1024)S(1)}, f32[4096]{0:T(1024)}, u32[]{:S(2)}) copy-start(f32[4096]{0:T(1024)} %param.32) | copy-start | bytes 49156
  63.1 143.2 %copy-start.13 = (bf16[512,512]{1,0:T(8,128)(2,1)S(1)}, bf16[512,512]{1,0:T(8,128)(2,1)}, u32[]{:S(2)}) copy-start(bf16[512,512]{1,0:T(8,128)(2,1)} %param.39) | copy-start | bytes 1572868
  63.1 143.2 %copy-start.14 = (bf16[512,512]{1,0:T(8,128)(2,1)S(1)}, bf16[512,512]{1,0:T(8,128)(2,1)}, u32[]{:S(2)}) copy-start(bf16[512,512]{1,0:T(8,128)(2,1)} %param.38) | copy-start | bytes 1572868
  148.2 60.0 %copy-start.10 = (s32[32,2]{0,1:T(2,128)S(1)}, s32[32,2]{0,1:T(2,128)}, u32[]{:S(2)}) copy-start(s32[32,2]{0,1:T(2,128)} %param.34) | copy-start | bytes 772
  148.2 90.2 %reduce-scatter.5.cloned.1.call-start = ((), (), s32[]{:S(2)}) async-start(), calls=%async_computation.9 | async-start | bytes 589824 | tf_op jit(solution)/shard_map/reduce_scatter | solution.py:134
  207.6 81.4 %all-gather.5.cloned.1.call-start = ((), (), s32[]{:S(2)}) async-start(), calls=%async_computation.10 | async-start | bytes 4718592 | tf_op jit(solution)/shard_map/all_gather | solution.py:147
  210.3 82.4 %all-to-all-start.1 = ((bf16[8,16,4096]{2,1,0:T(8,128)(2,1)}), bf16[8,16,4096]{2,1,0:T(8,128)(2,1)S(1)}, u32[]{:S(2)}, u32[]{:S(2)}) async-start(bf16[8,16,4096]{2,1,0:T(8,128)(2,1)} %bitcast.9), calls=%async_computation.2 | async-start | bytes 2097152 | tf_op jit(solution)/shard_map/all_to_all | solution.py:116
  213.9 143.0 %all-reduce.6.cloned.1.call-start = ((), (), s32[]{:S(2)}) async-start(), calls=%async_computation.11 | async-start | bytes 2621440 | tf_op jit(solution)/shard_map/psum | solution.py:123
  295.6 65.9 %copy-start.11 = (bf16[4096]{0:T(1024)(128)(2,1)S(1)}, bf16[4096]{0:T(1024)(128)(2,1)}, u32[]{:S(2)}) copy-start(bf16[4096]{0:T(1024)(128)(2,1)} %param.41) | copy-start | bytes 24580
  295.6 66.6 %copy-start.7 = (bf16[4096,8]{0,1:T(8,128)(2,1)S(1)}, bf16[4096,8]{0,1:T(8,128)(2,1)}, u32[]{:S(2)}) copy-start(bf16[4096,8]{0,1:T(8,128)(2,1)} %param.33) | copy-start | bytes 196612
  301.5 86.5 %copy-start.2 = (bf16[32,4096]{1,0:T(8,128)(2,1)S(1)}, bf16[32,4096]{1,0:T(8,128)(2,1)}, u32[]{:S(2)}) copy-start(bf16[32,4096]{1,0:T(8,128)(2,1)} %all-reduce.4.cloned.1.call-done) | copy-start | bytes 786436
  356.9 31.2 %all-to-all-start.2 = ((bf16[8,16,4096]{2,1,0:T(8,128)(2,1)}), bf16[8,16,4096]{2,1,0:T(8,128)(2,1)S(1)}, u32[]{:S(2)}, u32[]{:S(2)}) async-start(bf16[8,16,4096]{2,1,0:T(8,128)(2,1)} %get-tuple-element.3), calls=%async_computation.3 | async-start | bytes 2097152 | tf_op jit(solution)/shard_map/all_to_all | solution.py:124
Sparse Core Ops, SparseCore 0:
  29.1 31.6 reduce-scatter.2
  62.3 80.1 all-gather.2
  148.3 41.5 all-reduce.3
  207.7 30.6 reduce-scatter.4
  239.8 49.1 all-gather.4
  301.7 55.1 all-reduce.5
where the time goes:
time: 398 us; the launch traced here: 397 us
  waiting for transfers between devices  308 us (77%)
  blocking collectives  30.1 us (8%)
  matrix products  26.9 us (7%)
  between operations  14.4 us (4%)
  starting transfers between devices  8.4 us (2%)
  other arithmetic  6.59 us (2%)
    all_gather x1, waiting for transfers between devices, on_device(): lax.all_gather(out_weight, 'ep', axis=1, tiled=True)  79.5 us
    psum x1, waiting for transfers between devices, on_device(): total = lax.psum(partial_value.astype(jnp.bfloat16), 'tp')  55.4 us
    all_gather x1, waiting for transfers between devices, on_device(): lax.all_gather(dense_down, 'ep', axis=1, tiled=True)  49.8 us
    psum x1, waiting for transfers between devices, on_device(): lax.psum(mixer_part.astype(jnp.bfloat16), 'tp').astype(jnp.float32)  41.6 us
    reduce_scatter x1, waiting for transfers between devices, on_device(): lax.psum_scatter(jnp.dot(arrived, joined, preferred_element_type=jnp.floa...  30.9 us
    all_to_all x1, waiting for transfers between devices, on_device(): lax.all_to_all(total.reshape(sources, items, total.shape[1]), 'ep', split...  25.4 us
    reduce_scatter x1, waiting for transfers between devices, on_device(): lax.psum_scatter(jnp.dot(dense_arrived, dense_joined, preferred_element_t...  24.5 us
    all_to_all x1, blocking collectives, on_device(): lax.all_to_all(normed, 'ep', split_axis=1, concat_axis=0, tiled=True)  16 us
  transfers between devices with their start and end apart: 8, of which 7 were waited for; matrix products, arithmetic and copies ran while one was open for 3% of the time, Pallas kernels for 0%

commit v1 on v0

--- a/solution.py
+++ b/solution.py
@@ -72,7 +72,7 @@
     mixer_rows = (new_state * jax.nn.gelu(gate_branch.astype(jnp.float32))).astype(jnp.bfloat16)
     mixer_part = jnp.dot(
         mixer_rows,
-        lax.all_gather(out_weight, "ep", axis=1, tiled=True),
+        jnp.concatenate(lax.all_gather(out_weight, "ep"), axis=1),
         preferred_element_type=jnp.float32,
     )
     resid = (

time: 398 us -> 410 us (1.030)
  local copies, waits for them, and re-layouts: 2.18 us -> 13.6 us
    reshape x0 -> x1, local copies, waits for them, and re-layouts: none -> 11.5 us  [on_device(): jnp.concatenate(lax.all_gather(out_weight, 'ep'), axis=1)]
  transfers between devices with their start and end apart: 8 -> 8, of which waited for: 7 -> 7; matrix products, arithmetic and copies ran while one was open for 3% -> 2% of each run, Pallas kernels for 0% -> 0%
where the time goes in v1:
time: 410 us
  waiting for transfers between devices  308 us (75%)
  blocking collectives  30.1 us (7%)
  matrix products  28 us (7%)
  between operations  14.4 us (4%)
  local copies, waits for them, and re-layouts  13.6 us (3%)
  starting transfers between devices  8.4 us (2%)
  other arithmetic  6.59 us (2%)
    all_gather x1, waiting for transfers between devices, on_device(): lax.all_gather(out_weight, 'ep')  79.6 us
    psum x1, waiting for transfers between devices, on_device(): total = lax.psum(partial_value.astype(jnp.bfloat16), 'tp')  55.3 us
    all_gather x1, waiting for transfers between devices, on_device(): lax.all_gather(dense_down, 'ep', axis=1, tiled=True)  49.8 us
    psum x1, waiting for transfers between devices, on_device(): lax.psum(mixer_part.astype(jnp.bfloat16), 'tp').astype(jnp.float32)  41.6 us
    reduce_scatter x1, waiting for transfers between devices, on_device(): lax.psum_scatter(jnp.dot(arrived, joined, preferred_element_type=jnp.floa...  30.9 us
    all_to_all x1, waiting for transfers between devices, on_device(): lax.all_to_all(total.reshape(sources, items, total.shape[1]), 'ep', split...  25.4 us
    reduce_scatter x1, waiting for transfers between devices, on_device(): lax.psum_scatter(jnp.dot(dense_arrived, dense_joined, preferred_element_t...  24.5 us
    all_to_all x1, blocking collectives, on_device(): lax.all_to_all(normed, 'ep', split_axis=1, concat_axis=0, tiled=True)  16 us
  transfers between devices with their start and end apart: 8, of which 7 were waited for; matrix products, arithmetic and copies ran while one was open for 2% of the time, Pallas kernels for 0%

profile of v1, /device:TPU:0, one launch (start us, length us, event | category | flops | bytes accessed | tf_op | source)
XLA Modules:
  0.0 409.5 jit_solution(11488665345489946718)
XLA Ops:
  7.2 1.1 fusion.33
  8.4 1.1 fusion.35
  9.5 16.0 %all_to_all.48 = bf16[32,8,512]{2,0,1:T(8,128)(2,1)S(1)} all-to-all(bf16[32,8,512]{2,0,1:T(8,128)(2,1)S(1)} %bitcast.83), channel_id=1, replica_groups=mesh['ep'=8,'tp'=4] {'ep'}, dimensions={1} | all-to-all | bytes 524288 | tf_op jit(solution)/shard_map/all_to_all | solution.py:43
  25.5 3.4 convolution_convert_fusion.4
  29.0 0.7 all-gather.6.cloned.1.call-update
  29.7 30.9 %reduce-scatter.3.cloned.1.call-done = bf16[32,2048]{1,0:T(8,128)(2,1)} async-done(((bf16[256,2048]{1,0:T(8,128)(2,1)}), bf16[32,2048]{1,0:T(8,128)(2,1)}) %reduce-scatter.3.cloned.1.call-update) | async-done | bytes 131088 | tf_op jit(solution)/shard_map/reduce_scatter | solution.py:45
  60.7 0.8 slice_bitcast_fusion
  61.8 0.2 fusion.13
  62.3 0.2 fusion.17
  62.9 79.6 %all-gather.6.cloned.1.call-done = bf16[8192,512]{1,0:T(8,128)(2,1)} async-done(((bf16[1024,512]{1,0:T(8,128)(2,1)}), bf16[8192,512]{1,0:T(8,128)(2,1)}) %all-gather.6.cloned.1.call-update) | async-done | bytes 8388624 | tf_op jit(solution)/shard_map/all_gather | solution.py:75
  142.5 11.5 %copy.71 = bf16[1024,8,512]{0,2,1:T(8,128)(2,1)} copy(bf16[1024,8,512]{2,0,1:T(8,128)(2,1)} %bitcast.78) | data formatting | bytes 16777216 | tf_op jit(solution)/shard_map/reshape | solution.py:75
  154.0 6.7 %convolution_convert_fusion.3 = bf16[32,4096]{1,0:T(8,128)(2,1)} fusion(bf16[1024,4096]{0,1:T(8,128)(2,1)} %bitcast.75, f32[32,1024]{1,0:T(8,128)S(1)} %multiply_add_fusion, bf16[32,2048]{1,0:T(8,128)(2,1)S(1)} %copy-done.5), kind=kOutput, calls=%fused_computation.6 | convolution fusion | flops 268926976 | bytes 8847360 | tf_op jit(solution)/shard_map/dot_general | solution.py:73
  160.8 41.6 %all-reduce.4.cloned.1.call-done = bf16[32,4096]{1,0:T(8,128)(2,1)} async-done(((bf16[32,4096]{1,0:T(8,128)(2,1)}), bf16[32,4096]{1,0:T(8,128)(2,1)}) %all-reduce.4.cloned.1.call-update) | async-done | bytes 262160 | tf_op jit(solution)/shard_map/psum | solution.py:80
  202.5 1.1 fusion.37
  203.6 1.1 fusion.39
  204.7 14.1 %all_to_all.49 = bf16[32,8,512]{2,0,1:T(8,128)(2,1)S(1)} all-to-all(bf16[32,8,512]{2,0,1:T(8,128)(2,1)S(1)} %bitcast.84), channel_id=1, replica_groups=mesh['ep'=8,'tp'=4] {'ep'}, dimensions={1} | all-to-all | bytes 524288 | tf_op jit(solution)/shard_map/all_to_all | solution.py:132
  218.8 1.3 convolution_convert_fusion.5
  220.2 0.5 all-gather.4.cloned.1.call-update
  221.5 1.4 convolution_convert_fusion.1
  222.9 3.6 all-to-all-start.1
  226.5 24.5 %reduce-scatter.5.cloned.1.call-done = bf16[32,1024]{1,0:T(8,128)(2,1)} async-done(((bf16[256,1024]{1,0:T(8,128)(2,1)}), bf16[32,1024]{1,0:T(8,128)(2,1)}) %reduce-scatter.5.cloned.1.call-update) | async-done | bytes 65552 | tf_op jit(solution)/shard_map/reduce_scatter | solution.py:134
  251.0 0.8 convert_element_type.109
  251.8 49.8 %all-gather.4.cloned.1.call-done = bf16[512,4096]{1,0:T(8,128)(2,1)} async-done(((bf16[512,512]{1,0:T(8,128)(2,1)}), bf16[512,4096]{1,0:T(8,128)(2,1)}) %all-gather.4.cloned.1.call-update) | async-done | bytes 4194320 | tf_op jit(solution)/shard_map/all_gather | solution.py:147
  301.6 3.7 convolution_convert_fusion.2
  305.3 2.9 fusion.5
  308.2 5.9 %convolution_convert_fusion = bf16[128,4096]{1,0:T(8,128)(2,1)} fusion(bf16[1,512,4096]{2,1,0:T(8,128)(2,1)} %param.37, bf16[128,4096]{1,0:T(8,128)(2,1)S(1)} %bitcast.77, bf16[1,4096,512]{2,1,0:T(8,128)(2,1)} %param.36, f32[128,512]{1,0:T(8,128)S(1)} %fusion.5), kind=kOutput, calls=%fused_computation | convolution fusion | flops 1074659328 | bytes 10747904 | tf_op jit(solution)/shard_map/dot_general | solution.py:122
  314.2 55.3 %all-reduce.6.cloned.1.call-done = (bf16[8,16,4096]{2,1,0:T(8,128)(2,1)}, bf16[32,4096]{1,0:T(8,128)(2,1)}) async-done(((bf16[8,16,4096]{2,1,0:T(8,128)(2,1)}, bf16[32,4096]{1,0:T(8,128)(2,1)}), (bf16[8,16,4096]{2,1,0:T(8,128)(2,1)}, bf16[32,4096]{1,0:T(8,128)(2,1)})) %all-reduce.6.cloned.1.call-update) | async-done | bytes 1310736 | tf_op jit(solution)/shard_map/psum | solution.py:123
  369.5 4.6 %all-to-all-start.2 = ((bf16[8,16,4096]{2,1,0:T(8,128)(2,1)}), bf16[8,16,4096]{2,1,0:T(8,128)(2,1)S(1)}, u32[]{:S(2)}, u32[]{:S(2)}) async-start(bf16[8,16,4096]{2,1,0:T(8,128)(2,1)} %get-tuple-element.3), calls=%async_computation.3 | async-start | bytes 2097152 | tf_op jit(solution)/shard_map/all_to_all | solution.py:124
  374.1 0.7 fusion.45
  375.1 0.2 fusion.27
  375.3 25.4 %all-to-all-done.2 = bf16[8,16,4096]{2,1,0:T(8,128)(2,1)S(1)} async-done(((bf16[8,16,4096]{2,1,0:T(8,128)(2,1)}), bf16[8,16,4096]{2,1,0:T(8,128)(2,1)S(1)}, u32[]{:S(2)}, u32[]{:S(2)}) %all-to-all-start.2) | async-done | bytes 1048608 | tf_op jit(solution)/shard_map/all_to_all | solution.py:124
  400.7 2.0 fusion.1
  (70 shorter events, 2.3 us)
Async XLA Ops:
  7.2 54.6 %copy-start = (bf16[16,64,64]{2,1,0:T(8,128)(2,1)S(1)}, bf16[16,64,64]{2,1,0:T(8,128)(2,1)}, u32[]{:S(2)}) copy-start(bf16[16,64,64]{2,1,0:T(8,128)(2,1)} %param.29) | copy-start | bytes 393220
  7.2 53.5 %reduce-scatter.3.cloned.1.call-start = ((), (), s32[]{:S(2)}) async-start(), calls=%async_computation.6 | async-start | bytes 1179648 | tf_op jit(solution)/shard_map/reduce_scatter | solution.py:45
  8.4 21.3 %copy-start.12 = (f32[1024]{0:T(1024)S(1)}, f32[1024]{0:T(1024)}, u32[]{:S(2)}) copy-start(f32[1024]{0:T(1024)} %param.30) | copy-start | bytes 12292
  9.5 52.0 %copy-start.3 = (bf16[32,3,1024]{2,0,1:T(8,128)(2,1)S(1)}, bf16[32,3,1024]{2,0,1:T(8,128)(2,1)}, u32[]{:S(2)}) copy-start(bf16[32,3,1024]{2,0,1:T(8,128)(2,1)} %param.23) | copy-start | bytes 589828
  9.5 52.0 %copy-start.9 = (f32[4,1024]{1,0:T(4,128)S(1)}, f32[4,1024]{1,0:T(4,128)}, u32[]{:S(2)}) copy-start(f32[4,1024]{1,0:T(4,128)} %param.27) | copy-start | bytes 49156
  25.5 36.7 %copy-start.15 = (bf16[16,64,64]{2,1,0:T(8,128)(2,1)S(1)}, bf16[16,64,64]{2,1,0:T(8,128)(2,1)}, u32[]{:S(2)}) copy-start(bf16[16,64,64]{2,1,0:T(8,128)(2,1)} %param.28) | copy-start | bytes 393220
  28.9 33.9 %copy-start.6 = (f32[32,1024]{1,0:T(8,128)S(1)}, f32[32,1024]{1,0:T(8,128)}, u32[]{:S(2)}) copy-start(f32[32,1024]{1,0:T(8,128)} %param.22) | copy-start | bytes 393220
  28.9 113.6 %all-gather.6.cloned.1.call-start = ((), (), s32[]{:S(2)}) async-start(), calls=%async_computation.10 | async-start | bytes 9437184 | tf_op jit(solution)/shard_map/all_gather | solution.py:75
  29.7 172.8 %all-reduce.4.cloned.1.call-start = ((), (), s32[]{:S(2)}) async-start(), calls=%async_computation.7 | async-start | bytes 524288 | tf_op jit(solution)/shard_map/psum | solution.py:80
  62.9 91.0 %copy-start.4 = (f32[32,1024]{1,0:T(8,128)}, f32[32,1024]{1,0:T(8,128)S(1)}, u32[]{:S(2)}) copy-start(f32[32,1024]{1,0:T(8,128)S(1)} %multiply_add_fusion) | copy-start | bytes 393220
  142.5 11.5 %copy-start.5 = (bf16[32,2048]{1,0:T(8,128)(2,1)S(1)}, bf16[32,2048]{1,0:T(8,128)(2,1)}, u32[]{:S(2)}) copy-start(bf16[32,2048]{1,0:T(8,128)(2,1)} %reduce-scatter.3.cloned.1.call-done) | copy-start | bytes 393220
  154.0 48.5 %copy-start.1 = (bf16[32,4096]{1,0:T(8,128)(2,1)S(1)}, bf16[32,4096]{1,0:T(8,128)(2,1)}, u32[]{:S(2)}) copy-start(bf16[32,4096]{1,0:T(8,128)(2,1)} %param.21) | copy-start | bytes 786436
  154.0 49.6 %copy-start.8 = (f32[4096]{0:T(1024)S(1)}, f32[4096]{0:T(1024)}, u32[]{:S(2)}) copy-start(f32[4096]{0:T(1024)} %param.32) | copy-start | bytes 49156
  154.0 64.9 %copy-start.13 = (bf16[512,512]{1,0:T(8,128)(2,1)S(1)}, bf16[512,512]{1,0:T(8,128)(2,1)}, u32[]{:S(2)}) copy-start(bf16[512,512]{1,0:T(8,128)(2,1)} %param.39) | copy-start | bytes 1572868
  154.0 64.9 %copy-start.14 = (bf16[512,512]{1,0:T(8,128)(2,1)S(1)}, bf16[512,512]{1,0:T(8,128)(2,1)}, u32[]{:S(2)}) copy-start(bf16[512,512]{1,0:T(8,128)(2,1)} %param.38) | copy-start | bytes 1572868
  160.7 60.0 %copy-start.10 = (s32[32,2]{0,1:T(2,128)S(1)}, s32[32,2]{0,1:T(2,128)}, u32[]{:S(2)}) copy-start(s32[32,2]{0,1:T(2,128)} %param.34) | copy-start | bytes 772
  160.8 90.2 %reduce-scatter.5.cloned.1.call-start = ((), (), s32[]{:S(2)}) async-start(), calls=%async_computation.8 | async-start | bytes 589824 | tf_op jit(solution)/shard_map/reduce_scatter | solution.py:134
  220.1 81.4 %all-gather.4.cloned.1.call-start = ((), (), s32[]{:S(2)}) async-start(), calls=%async_computation.9 | async-start | bytes 4718592 | tf_op jit(solution)/shard_map/all_gather | solution.py:147
  222.9 82.4 %all-to-all-start.1 = ((bf16[8,16,4096]{2,1,0:T(8,128)(2,1)}), bf16[8,16,4096]{2,1,0:T(8,128)(2,1)S(1)}, u32[]{:S(2)}, u32[]{:S(2)}) async-start(bf16[8,16,4096]{2,1,0:T(8,128)(2,1)} %bitcast.12), calls=%async_computation.2 | async-start | bytes 2097152 | tf_op jit(solution)/shard_map/all_to_all | solution.py:116
  226.5 143.0 %all-reduce.6.cloned.1.call-start = ((), (), s32[]{:S(2)}) async-start(), calls=%async_computation.11 | async-start | bytes 2621440 | tf_op jit(solution)/shard_map/psum | solution.py:123
  308.2 65.9 %copy-start.11 = (bf16[4096]{0:T(1024)(128)(2,1)S(1)}, bf16[4096]{0:T(1024)(128)(2,1)}, u32[]{:S(2)}) copy-start(bf16[4096]{0:T(1024)(128)(2,1)} %param.41) | copy-start | bytes 24580
  308.2 66.6 %copy-start.7 = (bf16[4096,8]{0,1:T(8,128)(2,1)S(1)}, bf16[4096,8]{0,1:T(8,128)(2,1)}, u32[]{:S(2)}) copy-start(bf16[4096,8]{0,1:T(8,128)(2,1)} %param.33) | copy-start | bytes 196612
  314.1 86.5 %copy-start.2 = (bf16[32,4096]{1,0:T(8,128)(2,1)S(1)}, bf16[32,4096]{1,0:T(8,128)(2,1)}, u32[]{:S(2)}) copy-start(bf16[32,4096]{1,0:T(8,128)(2,1)} %all-reduce.4.cloned.1.call-done) | copy-start | bytes 786436
  369.5 31.2 %all-to-all-start.2 = ((bf16[8,16,4096]{2,1,0:T(8,128)(2,1)}), bf16[8,16,4096]{2,1,0:T(8,128)(2,1)S(1)}, u32[]{:S(2)}, u32[]{:S(2)}) async-start(bf16[8,16,4096]{2,1,0:T(8,128)(2,1)} %get-tuple-element.3), calls=%async_computation.3 | async-start | bytes 2097152 | tf_op jit(solution)/shard_map/all_to_all | solution.py:124
Sparse Core Ops, SparseCore 0:
  29.0 31.6 reduce-scatter.2
  62.3 80.1 all-gather.5
  160.9 41.5 all-reduce.3
  220.3 30.6 reduce-scatter.4
  252.4 49.1 all-gather.3
  314.3 55.1 all-reduce.5
